TPU v7x, 32 devices: a whole 2x2x4 slice. The times are simulated.
32 devices in a mesh: kv: 16 (over z, y, x), tp: 2 (over core).
Axes of the slice: x: 2, y: 2, z: 4, core: 2. Of those that a mesh axis runs over, the one named last changes fastest.
Arguments:
- tokens: bfloat16 [32, 4096], P(None, 'kv'), may hold values from -16 to 16
- mix_gain: bfloat16 [4096], P('kv'), may hold values from 0.099609375 to 1.8984375
- ffn_gain: bfloat16 [4096], P('kv'), may hold values from 0.099609375 to 1.8984375
- w_query: bfloat16 [4096, 2048], P('kv', 'tp'), may hold values from -0.09375 to 0.09375
- w_key: bfloat16 [4096, 2048], P('kv', 'tp'), may hold values from -0.09375 to 0.09375
- w_value: bfloat16 [4096, 4096], P('kv', 'tp'), may hold values from -0.09375 to 0.09375
- w_gate: bfloat16 [4096, 4096], P('kv', 'tp'), may hold values from -0.09375 to 0.09375
- w_decay: bfloat16 [4096, 2048], P('kv', 'tp'), may hold values from -0.375 to 0.375
- decay_bias: float32 [2048], P('tp'), may hold values from -7 to 4
- head_gain: bfloat16 [512], replicated, may hold values from 0.099609375 to 1.8984375
- w_output: bfloat16 [4096, 4096], P('tp', 'kv'), may hold values from -0.09375 to 0.09375
- w_ffgate: bfloat16 [4096, 11008], P('kv', 'tp'), may hold values from -0.09375 to 0.09375
- w_ffup: bfloat16 [4096, 11008], P('kv', 'tp'), may hold values from -0.09375 to 0.09375
- w_down: bfloat16 [11008, 4096], P('tp', 'kv'), may hold values from -0.0546875 to 0.0546875
- state: float32 [32, 8, 256, 512], P('kv', 'tp'), may hold values from -6 to 6
Outputs:
- mixed: bfloat16 [32, 4096], P(None, 'kv')
- new_state: float32 [32, 8, 256, 512], P('kv', 'tp')
All inputs are finite; a program needn't handle non-finite values.
Results may differ from a plain program's by a relative error of at most 0.015.
Values may be sent and summed in bfloat16 or wider, within the bound.
No kernel may reach another device: no remote copies, remote signals or barrier semaphores. Data moves between devices by JAX's collectives and lax.ppermute only.
A program may use at most 64 MiB of HBM per device.

v0:
```python
import jax
import jax.numpy as jnp
from jax import lax
from jax.sharding import PartitionSpec as P

epsilon = 1e-06


def local(
    tokens,
    mix_gain,
    ffn_gain,
    w_query,
    w_key,
    w_value,
    w_gate,
    w_decay,
    decay_bias,
    head_gain,
    w_output,
    w_ffgate,
    w_ffup,
    w_down,
    state,
):
    own_rows = state.shape[0]
    local_heads = state.shape[1]
    key_dim = state.shape[2]
    val_dim = state.shape[3]
    model_width = tokens.shape[1] * lax.axis_size("kv")
    row_offset = lax.axis_index("kv") * own_rows
    token_f32 = tokens.astype(jnp.float32)
    row_squares = jnp.sum(token_f32 * token_f32, axis=1)
    mix_in = (token_f32 * mix_gain.astype(jnp.float32)).astype(jnp.bfloat16)
    query_part = jnp.dot(mix_in, w_query, preferred_element_type=jnp.float32)
    key_part = jnp.dot(mix_in, w_key, preferred_element_type=jnp.float32)
    value_part = jnp.dot(mix_in, w_value, preferred_element_type=jnp.float32)
    gate_part = jnp.dot(mix_in, w_gate, preferred_element_type=jnp.float32)
    decay_part = jnp.dot(mix_in, w_decay, preferred_element_type=jnp.float32)
    square_total = lax.psum(row_squares, "kv")
    own_squares = lax.dynamic_slice_in_dim(square_total, row_offset, own_rows)
    query_sum, key_sum, value_sum, gate_sum, decay_sum = (
        lax.psum_scatter(query_part, "kv", scatter_dimension=0, tiled=True),
        lax.psum_scatter(key_part, "kv", scatter_dimension=0, tiled=True),
        lax.psum_scatter(value_part, "kv", scatter_dimension=0, tiled=True),
        lax.psum_scatter(gate_part, "kv", scatter_dimension=0, tiled=True),
        lax.psum_scatter(decay_part, "kv", scatter_dimension=0, tiled=True),
    )
    mix_rms = lax.rsqrt(own_squares / model_width + epsilon)[:, None]
    queries = (query_sum * mix_rms).reshape(own_rows, local_heads, key_dim) * key_dim ** (-0.5)
    key_rows = (key_sum * mix_rms).reshape(own_rows, local_heads, key_dim)
    value_rows = (value_sum * mix_rms).reshape(own_rows, local_heads, val_dim)
    gate_rows = (gate_sum * mix_rms).reshape(own_rows, local_heads, val_dim)
    decay_rows = (decay_sum * mix_rms + decay_bias).reshape(own_rows, local_heads, key_dim)
    log_decay = jax.nn.log_sigmoid(decay_rows) / 16.0
    new_state = (
        jnp.exp(log_decay)[..., None] * state + key_rows[..., :, None] * value_rows[..., None, :]
    )
    attended = jnp.einsum("bhk,bhkv->bhv", queries, new_state, precision=lax.Precision.HIGHEST)
    attended = attended * lax.rsqrt(
        jnp.sum(attended * attended, axis=2, keepdims=True) / val_dim + epsilon
    )
    head_out = (
        (attended * head_gain.astype(jnp.float32) * jax.nn.silu(gate_rows))
        .reshape(own_rows, local_heads * val_dim)
        .astype(jnp.bfloat16)
    )
    head_partial = jnp.dot(
        lax.all_gather(head_out, "kv", axis=0, tiled=True),
        w_output,
        preferred_element_type=jnp.float32,
    )
    attn_out = lax.psum(head_partial.astype(jnp.bfloat16), "tp").astype(jnp.float32)
    residual_mid = (token_f32 + attn_out).astype(jnp.bfloat16)
    mid_f32 = residual_mid.astype(jnp.float32)
    mid_squares = jnp.sum(mid_f32 * mid_f32, axis=1)
    ffn_in = (mid_f32 * ffn_gain.astype(jnp.float32)).astype(jnp.bfloat16)
    ffgate_part = jnp.dot(ffn_in, w_ffgate, preferred_element_type=jnp.float32)
    ffup_part = jnp.dot(ffn_in, w_ffup, preferred_element_type=jnp.float32)
    ffgate_sum, ffup_sum, square_sum = lax.psum((ffgate_part, ffup_part, mid_squares), "kv")
    ffn_rms = lax.rsqrt(square_sum / model_width + epsilon)[:, None]
    hidden = (jax.nn.silu(ffgate_sum * ffn_rms) * (ffup_sum * ffn_rms)).astype(jnp.bfloat16)
    down_part = jnp.dot(hidden, w_down, preferred_element_type=jnp.float32)
    ffn_out = lax.psum(down_part.astype(jnp.bfloat16), "tp").astype(jnp.float32)
    mixed = (mid_f32 + ffn_out).astype(jnp.bfloat16)
    return (mixed, new_state)


def solution(mesh):
    in_specs = (
        P(None, "kv"),
        P("kv"),
        P("kv"),
        P("kv", "tp"),
        P("kv", "tp"),
        P("kv", "tp"),
        P("kv", "tp"),
        P("kv", "tp"),
        P("tp"),
        P(),
        P("tp", "kv"),
        P("kv", "tp"),
        P("kv", "tp"),
        P("tp", "kv"),
        P("kv", "tp", None, None),
    )
    out_specs = (P(None, "kv"), P("kv", "tp", None, None))
    return jax.shard_map(local, mesh=mesh, in_specs=in_specs, out_specs=out_specs, check_vma=False)
```

profile of v0, /device:TPU:0, one launch (start us, length us, event | category | flops | bytes accessed | tf_op | source)
XLA Modules:
  0.0 317.6 jit_solution(6141432531111428591)
XLA Ops:
  7.2 0.0 copy-start
  7.2 0.0 copy-start.7
  7.2 0.0 copy-start.3
  7.2 0.0 copy-start.6
  7.2 0.0 copy-start.5
  7.2 0.0 copy-start.4
  7.2 0.0 all-reduce.12.cloned.1.call-start
  7.3 0.8 convert_element_type.49
  8.1 1.9 fusion.28
  10.0 1.9 fusion.26
  11.9 1.9 fusion.30
  13.9 2.2 fusion.24
  16.1 2.2 fusion.22
  18.3 0.0 all-reduce.12.cloned.1.call-update
  18.3 0.0 all-reduce.10.cloned.1.call-start
  18.4 0.0 copy-done.6
  18.4 0.0 copy-done.5
  18.5 0.0 copy-done.7
  18.5 0.6 dynamic-slice
  19.7 0.0 copy-done.3
  19.7 0.1 fusion.3
  19.8 43.7 %psum.42 = f32[32]{0:T(128)S(1)} all-reduce(f32[32]{0:T(128)S(1)} %fusion.3), channel_id=1, replica_groups=mesh['kv'=16,'tp'=2] {'kv'}, use_global_device_ids=true, to_apply=%region_2.0 | all-reduce | flops 32 | bytes 256 | tf_op jit(solution)/shard_map/psum | solution.py:40
  63.6 0.1 add_rsqrt_fusion.2
  63.6 70.8 %all-reduce.12.cloned.1.call-done = (f32[32,2048]{1,0:T(8,128)}, f32[32,1024]{1,0:T(8,128)}, f32[32,2048]{1,0:T(8,128)}, f32[32,1024]{1,0:T(8,128)}, f32[32,1024]{1,0:T(8,128)}) async-done(((f32[32,2048]{1,0:T(8,128)}, f32[32,1024]{1,0:T(8,128)}, f32[32,2048]{1,0:T(8,128)}, f32[32,1024]{1,0:T(8,128)}, f32[32,1024]{1,0:T(8,128)}), (f32[32,2048]{1,0:T(8,128)}, f32[32,1024]{1,0:T(8,128)}, ...) | async-done | bytes 917520
  134.4 0.0 copy-done.4
  134.4 0.9 fusion.20
  135.4 1.0 dynamic-slice_multiply_fusion.1
  136.4 2.6 multiply_add_fusion
  139.0 0.0 copy-start.1
  139.0 2.0 copy-done.1
  141.0 2.1 fusion.34
  143.1 0.1 fusion.9
  143.2 0.1 fusion.11
  143.3 39.5 %all-gather = bf16[16,2,2048]{2,1,0:T(2,128)(2,1)S(1)} all-gather(bf16[1,2,2048]{2,1,0:T(2,128)(2,1)S(1)} %reshape.47), channel_id=1, replica_groups=mesh['kv'=16,'tp'=2] {'kv'}, dimensions={0}, use_global_device_ids=true | all-gather | bytes 139264 | tf_op jit(solution)/shard_map/all_gather | solution.py:69
  182.9 0.1 reshape.48
  182.9 1.5 convolution_convert_fusion.1
  184.4 3.4 %psum.43 = bf16[32,256]{1,0:T(8,128)(2,1)S(1)} all-reduce(bf16[32,256]{1,0:T(8,128)(2,1)S(1)} %convolution_convert_fusion.1), channel_id=1, replica_groups=mesh['kv'=16,'tp'=2] {'tp'}, use_global_device_ids=true, to_apply=%region_8.9 | all-reduce | flops 8192 | bytes 32768 | tf_op jit(solution)/shard_map/psum | solution.py:73
  187.8 0.0 copy-start.2
  187.8 0.1 fusion.6
  187.9 0.0 copy-done
  187.9 1.5 fusion.12
  189.4 0.5 copy-done.2
  189.8 1.4 fusion.14
  191.3 0.0 all-reduce.10.cloned.1.call-update
  191.3 36.9 %psum.45 = f32[32]{0:T(128)S(1)} all-reduce(f32[32]{0:T(128)S(1)} %get-tuple-element.9), channel_id=1, replica_groups=mesh['kv'=16,'tp'=2] {'kv'}, use_global_device_ids=true, to_apply=%region_11.12 | all-reduce | flops 32 | bytes 256 | tf_op jit(solution)/shard_map/psum | solution.py:80
  228.2 75.7 %all-reduce.10.cloned.1.call-done = (f32[32,5504]{1,0:T(8,128)}, f32[32,5504]{1,0:T(8,128)}) async-done(((f32[32,5504]{1,0:T(8,128)}, f32[32,5504]{1,0:T(8,128)}), (f32[32,5504]{1,0:T(8,128)}, f32[32,5504]{1,0:T(8,128)})) %all-reduce.10.cloned.1.call-update) | async-done | bytes 1409040 | tf_op jit(solution)/shard_map/psum | solution.py:80
  303.9 2.8 convolution_convert_fusion
  306.8 3.4 %psum.47 = bf16[32,256]{1,0:T(8,128)(2,1)S(1)} all-reduce(bf16[32,256]{1,0:T(8,128)(2,1)S(1)} %convolution_convert_fusion), channel_id=1, replica_groups=mesh['kv'=16,'tp'=2] {'tp'}, use_global_device_ids=true, to_apply=%region_13.14 | all-reduce | flops 8192 | bytes 32768 | tf_op jit(solution)/shard_map/psum | solution.py:84
  310.1 0.6 fusion.7
  (11 shorter events, 0.2 us)
Async XLA Ops:
  7.2 180.7 %copy-start = (bf16[256,5504]{1,0:T(8,128)(2,1)S(1)}, bf16[256,5504]{1,0:T(8,128)(2,1)}, u32[]{:S(2)}) copy-start(bf16[256,5504]{1,0:T(8,128)(2,1)} %param.27) | copy-start | bytes 8454148
  7.2 11.3 %copy-start.7 = (u32[32]{0:T(128)S(1)}, u32[32]{0:T(128)}, u32[]{:S(2)}) copy-start(u32[32]{0:T(128)} %constant.41) | copy-start | bytes 388
  7.2 12.5 %copy-start.3 = (bf16[32,256]{1,0:T(8,128)(2,1)S(1)}, bf16[32,256]{1,0:T(8,128)(2,1)}, u32[]{:S(2)}) copy-start(bf16[32,256]{1,0:T(8,128)(2,1)} %param.15) | copy-start | bytes 49156
  7.2 11.2 %copy-start.6 = (bf16[256]{0:T(256)(128)(2,1)S(1)}, bf16[256]{0:T(256)(128)(2,1)}, u32[]{:S(2)}) copy-start(bf16[256]{0:T(256)(128)(2,1)} %param.17) | copy-start | bytes 1540
  7.2 11.2 %copy-start.5 = (bf16[512]{0:T(512)(128)(2,1)S(1)}, bf16[512]{0:T(512)(128)(2,1)}, u32[]{:S(2)}) copy-start(bf16[512]{0:T(512)(128)(2,1)} %param.24) | copy-start | bytes 3076
  7.2 127.2 %copy-start.4 = (f32[1024]{0:T(1024)S(1)}, f32[1024]{0:T(1024)}, u32[]{:S(2)}) copy-start(f32[1024]{0:T(1024)} %param.23) | copy-start | bytes 12292
  7.2 127.2 %all-reduce.12.cloned.1.call-start = ((), (), s32[]{:S(2)}) async-start(), calls=%async_computation.1 | async-start | bytes 1835008
  18.3 285.6 %all-reduce.10.cloned.1.call-start = ((), (), s32[]{:S(2)}) async-start(), calls=%async_computation | async-start | bytes 2818048 | tf_op jit(solution)/shard_map/psum | solution.py:80
  139.0 2.0 copy-start.1
  187.8 2.1 copy-start.2
Sparse Core Ops, SparseCore 0:
  18.5 115.9 all-reduce.11
  191.4 112.4 all-reduce.9
where the time goes:
time: 318 us
  waiting for transfers between devices  147 us (46%)
  blocking collectives  127 us (40%)
  matrix products  19.6 us (6%)
  between operations  14.9 us (5%)
  other arithmetic  6.37 us (2%)
  local copies, waits for them, and re-layouts  3.25 us (1%)
    psum x1, waiting for transfers between devices, local(): lax.psum((ffgate_part, ffup_part, mid_squares), 'kv')  75.7 us
    unnamed x3, waiting for transfers between devices  70.8 us
    psum x1, blocking collectives, local(): square_total = lax.psum(row_squares, 'kv')  43.7 us
    all_gather x1, blocking collectives, local(): lax.all_gather(head_out, 'kv', axis=0, tiled=True)  39.5 us
    psum x1, blocking collectives, local(): lax.psum((ffgate_part, ffup_part, mid_squares), 'kv')  36.9 us
  transfers between devices with their start and end apart: 2, of which 2 were waited for; matrix products, arithmetic and copies ran while one was open for 0% of the time, Pallas kernels for 0%

commit v1 on v0

--- a/solution.py
+++ b/solution.py
@@ -4,6 +4,13 @@
 from jax.sharding import PartitionSpec as P
 
 epsilon = 1e-06
+
+
+def _create_counts(z):
+    part_now = lax.axis_size("kv")
+    x_now = jnp.stack([z] * part_now, 0)
+    response = lax.all_to_all(x_now, "kv", 0, 0)
+    return jnp.concatenate(response, 0)
 
 
 def local(
@@ -65,11 +72,7 @@
         .reshape(own_rows, local_heads * val_dim)
         .astype(jnp.bfloat16)
     )
-    head_partial = jnp.dot(
-        lax.all_gather(head_out, "kv", axis=0, tiled=True),
-        w_output,
-        preferred_element_type=jnp.float32,
-    )
+    head_partial = jnp.dot(_create_counts(head_out), w_output, preferred_element_type=jnp.float32)
     attn_out = lax.psum(head_partial.astype(jnp.bfloat16), "tp").astype(jnp.float32)
     residual_mid = (token_f32 + attn_out).astype(jnp.bfloat16)
     mid_f32 = residual_mid.astype(jnp.float32)

time: 318 us -> 293 us (0.921)
  blocking collectives: 127 us -> 88.8 us
  waiting for transfers between devices: 147 us -> 154 us
  starting transfers between devices: 0.08 us -> 4.84 us
    all_gather x1 -> x0, blocking collectives: 39.5 us -> none  [local(): lax.all_gather(head_out, 'kv', axis=0, tiled=True)]
    all_to_all x0 -> x1, waiting for transfers between devices: none -> 7.72 us  [_create_counts(): response = lax.all_to_all(x_now, 'kv', 0, 0)]
    all_to_all x0 -> x1, starting transfers between devices: none -> 4.76 us  [_create_counts(): response = lax.all_to_all(x_now, 'kv', 0, 0)]
  transfers between devices with their start and end apart: 2 -> 3, of which waited for: 2 -> 3; matrix products, arithmetic and copies ran while one was open for 0% -> 0% of each run, Pallas kernels for 0% -> 0%
where the time goes in v1:
time: 293 us; the launch traced here: 292 us
  waiting for transfers between devices  154 us (53%)
  blocking collectives  88.8 us (30%)
  matrix products  19.6 us (7%)
  between operations  14.9 us (5%)
  other arithmetic  6.37 us (2%)
  starting transfers between devices  4.84 us (2%)
  local copies, waits for them, and re-layouts  3.96 us (1%)
    psum x1, waiting for transfers between devices, local(): lax.psum((ffgate_part, ffup_part, mid_squares), 'kv')  75.1 us
    unnamed x3, waiting for transfers between devices  70.9 us
    psum x1, blocking collectives, local(): square_total = lax.psum(row_squares, 'kv')  43.9 us
    psum x1, blocking collectives, local(): lax.psum((ffgate_part, ffup_part, mid_squares), 'kv')  38.2 us
    all_to_all x1, waiting for transfers between devices, _create_counts(): response = lax.all_to_all(x_now, 'kv', 0, 0)  7.72 us
  transfers between devices with their start and end apart: 3, of which 3 were waited for; matrix products, arithmetic and copies ran while one was open for 0% of the time, Pallas kernels for 0%

profile of v1, /device:TPU:0, one launch (start us, length us, event | category | flops | bytes accessed | tf_op | source)
XLA Modules:
  0.0 292.1 jit_solution(14878677402918972135)
XLA Ops:
  7.2 0.0 copy-start
  7.2 0.0 copy-start.7
  7.2 0.0 copy-start.3
  7.2 0.0 copy-start.5
  7.2 0.0 copy-start.4
  7.2 0.0 all-reduce.12.cloned.1.call-start
  7.3 0.8 convert_element_type.51
  8.1 1.9 fusion.29
  10.0 1.9 fusion.27
  11.9 1.9 fusion.31
  13.8 2.2 fusion.25
  16.1 2.2 fusion.23
  18.3 0.0 all-reduce.12.cloned.1.call-update
  18.3 0.0 copy-done.5
  18.4 0.0 copy-done.7
  18.4 0.6 dynamic-slice
  19.6 0.0 copy-done.3
  19.6 0.1 fusion.3
  19.7 43.9 %psum.42 = f32[32]{0:T(128)S(1)} all-reduce(f32[32]{0:T(128)S(1)} %fusion.3), channel_id=1, replica_groups=mesh['kv'=16,'tp'=2] {'kv'}, use_global_device_ids=true, to_apply=%region_2.0 | all-reduce | flops 32 | bytes 256 | tf_op jit(solution)/shard_map/psum | solution.py:47
  63.6 0.1 add_rsqrt_fusion.2
  63.7 70.9 %all-reduce.12.cloned.1.call-done = (f32[32,2048]{1,0:T(8,128)}, f32[32,1024]{1,0:T(8,128)}, f32[32,2048]{1,0:T(8,128)}, f32[32,1024]{1,0:T(8,128)}, f32[32,1024]{1,0:T(8,128)}) async-done(((f32[32,2048]{1,0:T(8,128)}, f32[32,1024]{1,0:T(8,128)}, f32[32,2048]{1,0:T(8,128)}, f32[32,1024]{1,0:T(8,128)}, f32[32,1024]{1,0:T(8,128)}), (f32[32,2048]{1,0:T(8,128)}, f32[32,1024]{1,0:T(8,128)}, ...) | async-done | bytes 917520
  134.6 0.0 copy-done.4
  134.6 0.9 fusion.20
  135.5 1.0 dynamic-slice_multiply_fusion.1
  136.6 2.6 multiply_add_fusion
  139.2 0.0 copy-start.1
  139.2 2.0 copy-done.1
  141.2 0.0 copy-start.6
  141.2 2.1 fusion.35
  143.2 0.1 fusion.9
  143.4 0.1 fusion.22
  143.5 0.7 stack.2
  144.2 4.8 %all-to-all-start = ((bf16[16,2,2048]{2,1,0:T(2,128)(2,1)}), bf16[16,2,2048]{2,1,0:T(2,128)(2,1)S(1)}, u32[]{:S(2)}, u32[]{:S(2)}) async-start(bf16[16,2,2048]{2,1,0:T(2,128)(2,1)} %stack.2), calls=%async_computation | async-start | bytes 262144 | tf_op jit(solution)/shard_map/all_to_all | solution.py:12
  148.9 0.0 all-reduce.10.cloned.1.call-start
  149.0 0.0 copy-done.6
  149.0 7.7 %all-to-all-done = bf16[16,2,2048]{2,1,0:T(2,128)(2,1)S(1)} async-done(((bf16[16,2,2048]{2,1,0:T(2,128)(2,1)}), bf16[16,2,2048]{2,1,0:T(2,128)(2,1)S(1)}, u32[]{:S(2)}, u32[]{:S(2)}) %all-to-all-start) | async-done | bytes 131104 | tf_op jit(solution)/shard_map/all_to_all | solution.py:12
  156.7 0.1 reshape.53
  156.8 1.5 convolution_convert_fusion.1
  158.3 3.4 %psum.43 = bf16[32,256]{1,0:T(8,128)(2,1)S(1)} all-reduce(bf16[32,256]{1,0:T(8,128)(2,1)S(1)} %convolution_convert_fusion.1), channel_id=1, replica_groups=mesh['kv'=16,'tp'=2] {'tp'}, use_global_device_ids=true, to_apply=%region_8.9 | all-reduce | flops 8192 | bytes 32768 | tf_op jit(solution)/shard_map/psum | solution.py:76
  161.6 0.0 copy-start.2
  161.7 0.1 fusion.6
  161.8 0.0 copy-done
  161.8 1.5 fusion.12
  163.2 0.5 copy-done.2
  163.7 1.4 fusion.14
  165.2 0.0 all-reduce.10.cloned.1.call-update
  165.2 38.2 %psum.45 = f32[32]{0:T(128)S(1)} all-reduce(f32[32]{0:T(128)S(1)} %get-tuple-element.9), channel_id=1, replica_groups=mesh['kv'=16,'tp'=2] {'kv'}, use_global_device_ids=true, to_apply=%region_11.12 | all-reduce | flops 32 | bytes 256 | tf_op jit(solution)/shard_map/psum | solution.py:83
  203.4 75.1 %all-reduce.10.cloned.1.call-done = (f32[32,5504]{1,0:T(8,128)}, f32[32,5504]{1,0:T(8,128)}) async-done(((f32[32,5504]{1,0:T(8,128)}, f32[32,5504]{1,0:T(8,128)}), (f32[32,5504]{1,0:T(8,128)}, f32[32,5504]{1,0:T(8,128)})) %all-reduce.10.cloned.1.call-update) | async-done | bytes 1409040 | tf_op jit(solution)/shard_map/psum | solution.py:83
  278.4 2.8 convolution_convert_fusion
  281.3 3.4 %psum.47 = bf16[32,256]{1,0:T(8,128)(2,1)S(1)} all-reduce(bf16[32,256]{1,0:T(8,128)(2,1)S(1)} %convolution_convert_fusion), channel_id=1, replica_groups=mesh['kv'=16,'tp'=2] {'tp'}, use_global_device_ids=true, to_apply=%region_13.14 | all-reduce | flops 8192 | bytes 32768 | tf_op jit(solution)/shard_map/psum | solution.py:87
  284.6 0.6 fusion.7
  (11 shorter events, 0.2 us)
Async XLA Ops:
  7.2 154.6 %copy-start = (bf16[256,5504]{1,0:T(8,128)(2,1)S(1)}, bf16[256,5504]{1,0:T(8,128)(2,1)}, u32[]{:S(2)}) copy-start(bf16[256,5504]{1,0:T(8,128)(2,1)} %param.27) | copy-start | bytes 8454148
  7.2 11.2 %copy-start.7 = (u32[32]{0:T(128)S(1)}, u32[32]{0:T(128)}, u32[]{:S(2)}) copy-start(u32[32]{0:T(128)} %constant.41) | copy-start | bytes 388
  7.2 12.4 %copy-start.3 = (bf16[32,256]{1,0:T(8,128)(2,1)S(1)}, bf16[32,256]{1,0:T(8,128)(2,1)}, u32[]{:S(2)}) copy-start(bf16[32,256]{1,0:T(8,128)(2,1)} %param.15) | copy-start | bytes 49156
  7.2 11.1 %copy-start.5 = (bf16[512]{0:T(512)(128)(2,1)S(1)}, bf16[512]{0:T(512)(128)(2,1)}, u32[]{:S(2)}) copy-start(bf16[512]{0:T(512)(128)(2,1)} %param.24) | copy-start | bytes 3076
  7.2 127.4 %copy-start.4 = (f32[1024]{0:T(1024)S(1)}, f32[1024]{0:T(1024)}, u32[]{:S(2)}) copy-start(f32[1024]{0:T(1024)} %param.23) | copy-start | bytes 12292
  7.2 127.3 %all-reduce.12.cloned.1.call-start = ((), (), s32[]{:S(2)}) async-start(), calls=%async_computation.2 | async-start | bytes 1835008
  139.2 2.0 copy-start.1
  141.2 7.8 %copy-start.6 = (bf16[256]{0:T(256)(128)(2,1)S(1)}, bf16[256]{0:T(256)(128)(2,1)}, u32[]{:S(2)}) copy-start(bf16[256]{0:T(256)(128)(2,1)} %param.17) | copy-start | bytes 1540
  144.2 12.6 %all-to-all-start = ((bf16[16,2,2048]{2,1,0:T(2,128)(2,1)}), bf16[16,2,2048]{2,1,0:T(2,128)(2,1)S(1)}, u32[]{:S(2)}, u32[]{:S(2)}) async-start(bf16[16,2,2048]{2,1,0:T(2,128)(2,1)} %stack.2), calls=%async_computation | async-start | bytes 262144 | tf_op jit(solution)/shard_map/all_to_all | solution.py:12
  148.9 129.5 %all-reduce.10.cloned.1.call-start = ((), (), s32[]{:S(2)}) async-start(), calls=%async_computation.1 | async-start | bytes 2818048 | tf_op jit(solution)/shard_map/psum | solution.py:83
  161.6 2.1 copy-start.2
Sparse Core Ops, SparseCore 0:
  18.5 116.0 all-reduce.11
  165.3 113.0 all-reduce.9
